TPU v7x, 32 devices: a whole 2x2x4 slice. The times are simulated.
32 devices in a mesh: sp: 8 (over z, x), tp: 4 (over y, core).
Axes of the slice: x: 2, y: 2, z: 4, core: 2. Of those that a mesh axis runs over, the one named last changes fastest.
Arguments:
- tokens: bfloat16 [2048, 3072], P('sp', 'tp'), may hold values from -6 to 6
- norm_gain: float32 [3072], replicated, may hold values from 0.1 to 1.9
- state_in_weight: bfloat16 [3072, 1024], P('sp', 'tp'), may hold values from -0.109375 to 0.109375
- pool_in_weight: bfloat16 [3072, 1024], P('sp', 'tp'), may hold values from -0.109375 to 0.109375
- rate_real: float32 [64, 64], replicated, may hold values from -1.5 to -0.5
- rate_imag: float32 [64, 64], replicated, may hold values from 0 to 200
- log_step: float32 [64], replicated, may hold values from -2 to 0.7
- input_real: float32 [64, 64, 16], replicated, may hold values from -1 to 1
- input_imag: float32 [64, 64, 16], replicated, may hold values from -1 to 1
- output_real: float32 [64, 16, 64], replicated, may hold values from -64 to 64
- output_imag: float32 [64, 16, 64], replicated, may hold values from -64 to 64
- skip_gain: float32 [1024], replicated, may hold values from -3 to 3
- pool_weight: bfloat16 [16, 64, 64], replicated, may hold values from -0.75 to 0.75
- pool_gain: float32 [1024], replicated, may hold values from 0.1 to 1.9
- state_out_weight: bfloat16 [1024, 3072], P('sp', 'tp'), may hold values from -0.125 to 0.125
- pool_out_weight: bfloat16 [1024, 3072], P('sp', 'tp'), may hold values from -0.125 to 0.125
Outputs:
- mixer_output: bfloat16 [2048, 3072], P('sp', 'tp')
All inputs are finite; a program needn't handle non-finite values.
Results may differ from a plain program's by a relative error of at most 0.0065.
Values may be sent and summed in bfloat16 or wider, within the bound.
A program may use at most 64 MiB of HBM per device.

v0:
```python
import jax
import jax.numpy as jnp
from jax import lax
from jax.sharding import PartitionSpec as P

SSM_GROUP = 16
POOL_GROUP = 64
epsilon = 1e-06
highest = lax.Precision.HIGHEST
window_reach = 16


def prefix(part, axis, combine, identity):
    place = lax.axis_index(axis)
    gathered = jax.tree.map(lambda a: lax.all_gather(a, axis), part)
    state = jax.tree.map(lambda a, e: jnp.zeros_like(a) + jnp.asarray(e, a.dtype), part, identity)

    def one(turn, state):
        return combine(
            state, jax.tree.map(lambda a: lax.dynamic_index_in_dim(a, turn, 0, False), gathered)
        )

    return lax.fori_loop(0, place, one, state)


def passed_along(value, axis, steps):
    count = lax.axis_size(axis)
    first, last = (max(0, -steps), min(count, count - steps))
    return lax.ppermute(value, axis, [(source, source + steps) for source in range(first, last)])


def discretize(rate_real, rate_imag, log_step, length):
    step_size = jnp.exp(log_step)[:, None] / length
    exponent = rate_real * step_size
    angle = rate_imag * step_size
    magnitude = jnp.exp(exponent)
    decay_real = magnitude * jnp.cos(angle)
    decay_imag = magnitude * jnp.sin(angle)
    less_one = jnp.expm1(exponent) * jnp.cos(angle) - 2.0 * jnp.square(jnp.sin(0.5 * angle))
    denominator = rate_real * rate_real + rate_imag * rate_imag
    factor_real = (less_one * rate_real + decay_imag * rate_imag) / denominator
    factor_imag = (decay_imag * rate_real - less_one * rate_imag) / denominator
    return (exponent, angle, decay_real, decay_imag, factor_real, factor_imag)


def complex_product(left_pair, right_pair):
    return jnp.stack(
        [
            left_pair[0] * right_pair[0] - left_pair[1] * right_pair[1],
            left_pair[0] * right_pair[1] + left_pair[1] * right_pair[0],
        ]
    )


def scan_combine(first_part, second_part):
    first_decay_real, first_decay_imag, first_real, first_imag = first_part
    second_decay_real, second_decay_imag, second_real, second_imag = second_part
    return (
        first_decay_real * second_decay_real - first_decay_imag * second_decay_imag,
        first_decay_real * second_decay_imag + first_decay_imag * second_decay_real,
        second_decay_real * first_real - second_decay_imag * first_imag + second_real,
        second_decay_real * first_imag + second_decay_imag * first_real + second_imag,
    )


def chain_combine(earlier, later):
    return (complex_product(later[0], earlier[0]), complex_product(later[0], earlier[1]) + later[1])


def local_slice(array, first_index, count_here):
    return lax.dynamic_slice_in_dim(array, first_index, count_here, 0)


def body(
    tokens,
    norm_gain,
    state_in_weight,
    pool_in_weight,
    rate_real,
    rate_imag,
    log_step,
    input_real,
    input_imag,
    output_real,
    output_imag,
    skip_gain,
    pool_weight,
    pool_gain,
    state_out_weight,
    pool_out_weight,
):
    state_in_full, pool_in_full, state_out_full, pool_out_full = (
        lax.all_gather(state_in_weight, "sp", axis=0, tiled=True),
        lax.all_gather(pool_in_weight, "sp", axis=0, tiled=True),
        lax.all_gather(state_out_weight, "sp", axis=0, tiled=True),
        lax.all_gather(pool_out_weight, "sp", axis=0, tiled=True),
    )
    row_count = tokens.shape[0]
    model_width = norm_gain.shape[0]
    state_width = state_in_full.shape[1]
    pool_width = pool_in_full.shape[1]
    features = lax.all_gather(tokens, "tp", axis=1, tiled=True).astype(jnp.float32)
    scaled = (features * norm_gain).astype(jnp.bfloat16)
    state_rows = state_in_full
    pool_rows = pool_in_full
    state_sum = jnp.dot(scaled, state_rows, preferred_element_type=jnp.float32)
    pool_sum = jnp.dot(scaled, pool_rows, preferred_element_type=jnp.float32)
    squares = jnp.sum(features * features, axis=1)
    state_sum, pool_sum, squares = (state_sum, pool_sum, squares)
    inverse = lax.rsqrt(squares / model_width + epsilon)[:, None]
    state_in = (state_sum * inverse).astype(jnp.bfloat16)
    pool_in = (pool_sum * inverse).astype(jnp.bfloat16)
    head_index = lax.axis_index("tp")
    block_index = lax.axis_index("sp")
    groups_here = state_width // SSM_GROUP
    first_group = head_index * groups_here
    length = row_count * lax.axis_size("sp")
    exponent, angle, decay_real, decay_imag, factor_real, factor_imag = discretize(
        local_slice(rate_real, first_group, groups_here),
        local_slice(rate_imag, first_group, groups_here),
        local_slice(log_step, first_group, groups_here),
        length,
    )
    state_columns = groups_here * decay_real.shape[1]
    exponent = exponent.reshape(state_columns)
    angle = angle.reshape(state_columns)
    decay_real = decay_real.reshape(state_columns)
    decay_imag = decay_imag.reshape(state_columns)
    group_identity = jnp.eye(groups_here, dtype=jnp.float32)
    local_in_real = local_slice(input_real, first_group, groups_here)
    local_in_imag = local_slice(input_imag, first_group, groups_here)
    drive_real = factor_real[..., None] * local_in_real - factor_imag[..., None] * local_in_imag
    drive_imag = factor_real[..., None] * local_in_imag + factor_imag[..., None] * local_in_real
    drive_matrix_real = jnp.einsum("gnc,gh->gchn", drive_real, group_identity).reshape(
        state_width, state_columns
    )
    drive_matrix_imag = jnp.einsum("gnc,gh->gchn", drive_imag, group_identity).reshape(
        state_width, state_columns
    )
    signal = state_in.astype(jnp.float32)
    push_real = jnp.dot(signal, drive_matrix_real, precision=highest)
    push_imag = jnp.dot(signal, drive_matrix_imag, precision=highest)
    decay_wide_real = jnp.broadcast_to(decay_real, push_real.shape)
    decay_wide_imag = jnp.broadcast_to(decay_imag, push_real.shape)
    _, _, local_real, local_imag = lax.associative_scan(
        scan_combine, (decay_wide_real, decay_wide_imag, push_real, push_imag), axis=0
    )
    end_state = jnp.stack([local_real[row_count - 1], local_imag[row_count - 1]])
    block_magnitude = jnp.exp(row_count * exponent)
    block_decay = jnp.stack(
        [block_magnitude * jnp.cos(row_count * angle), block_magnitude * jnp.sin(row_count * angle)]
    )
    last_rows = pool_in[row_count - window_reach :]
    identity = (
        jnp.stack([jnp.ones_like(exponent), jnp.zeros_like(exponent)]),
        jnp.zeros_like(end_state),
    )
    _, incoming = prefix((block_decay, end_state), "sp", chain_combine, identity)
    halo_block = passed_along(last_rows, "sp", 1)
    positions = (jnp.arange(row_count, dtype=jnp.float32) + 1.0)[:, None]
    power_magnitude = jnp.exp(positions * exponent[None, :])
    power_angle = positions * angle[None, :]
    power_cos = power_magnitude * jnp.cos(power_angle)
    power_sin = power_magnitude * jnp.sin(power_angle)
    states_real = local_real + power_cos * incoming[0] - power_sin * incoming[1]
    states_imag = local_imag + power_cos * incoming[1] + power_sin * incoming[0]
    local_out_real = local_slice(output_real, first_group, groups_here)
    local_out_imag = local_slice(output_imag, first_group, groups_here)
    read_matrix_real = jnp.einsum("gcn,gh->hngc", local_out_real, group_identity).reshape(
        state_columns, state_width
    )
    read_matrix_imag = jnp.einsum("gcn,gh->hngc", local_out_imag, group_identity).reshape(
        state_columns, state_width
    )
    readout_sum = jnp.dot(states_real, read_matrix_real, precision=highest)
    readout_sum = readout_sum - jnp.dot(states_imag, read_matrix_imag, precision=highest)
    readout_sum = (
        readout_sum + local_slice(skip_gain, head_index * state_width, state_width) * signal
    )
    state_out = jax.nn.gelu(readout_sum).astype(jnp.bfloat16)
    pool_groups_here = pool_width // POOL_GROUP
    first_pool = head_index * pool_groups_here
    extended = jnp.concatenate([halo_block, pool_in], axis=0)
    column_group = first_pool + jnp.arange(pool_width, dtype=jnp.int32) // POOL_GROUP
    column_window = jnp.left_shift(jnp.ones_like(column_group), column_group % 4 + 1)
    targets = jnp.arange(row_count, dtype=jnp.int32)[:, None] + window_reach
    sources = jnp.arange(row_count + window_reach, dtype=jnp.int32)[None, :]
    window_sums = jnp.zeros((row_count, pool_width), jnp.float32)
    for power_index in range(1, 5):
        span_width = 2**power_index
        band_mask = ((sources <= targets) & (sources > targets - span_width)).astype(jnp.bfloat16)
        partial_sums = jnp.dot(band_mask, extended, preferred_element_type=jnp.float32)
        window_sums = jnp.where(column_window[None, :] == span_width, partial_sums, window_sums)
    global_rows = block_index * row_count + jnp.arange(row_count, dtype=jnp.int32)
    divisor = jnp.minimum(global_rows[:, None] + 1, column_window[None, :]).astype(jnp.float32)
    pooled = window_sums / divisor - pool_in.astype(jnp.float32)
    pool_identity = jnp.eye(pool_groups_here, dtype=jnp.float32)
    mixer_matrix = jnp.einsum(
        "gcd,gh->gchd",
        local_slice(pool_weight, first_pool, pool_groups_here).astype(jnp.float32),
        pool_identity,
    ).reshape(pool_width, pool_width)
    projected = jnp.dot(pooled, mixer_matrix, precision=highest)
    pool_out = (projected * local_slice(pool_gain, head_index * pool_width, pool_width)).astype(
        jnp.bfloat16
    )
    state_rows = state_out_full
    pool_rows = pool_out_full
    running_sum = jnp.dot(
        lax.all_gather(state_out, "tp", axis=1, tiled=True),
        state_rows,
        preferred_element_type=jnp.float32,
    )
    combined = running_sum + jnp.dot(
        lax.all_gather(pool_out, "tp", axis=1, tiled=True),
        pool_rows,
        preferred_element_type=jnp.float32,
    )
    return combined.astype(jnp.bfloat16)


def solution(mesh):
    return jax.shard_map(
        body,
        mesh=mesh,
        in_specs=(
            P("sp", "tp"),
            P(),
            P("sp", "tp"),
            P("sp", "tp"),
            P(),
            P(),
            P(),
            P(),
            P(),
            P(),
            P(),
            P(),
            P(),
            P(),
            P("sp", "tp"),
            P("sp", "tp"),
        ),
        out_specs=P("sp", "tp"),
        check_vma=False,
    )
```

profile of v0, /device:TPU:25, one launch (start us, length us, event | category | flops | bytes accessed | tf_op | source)
XLA Modules:
  0.0 252.3 jit_solution(12776405410376965267)
XLA Ops:
  18.1 1.9 multiply_bitcast_fusion
  20.0 2.8 %reshape.307 = f32[1024,256]{0,1:T(8,128)} reshape(f32[16,64,16,16]{1,0,3,2:T(8,128)} %get-tuple-element.121) | data formatting | bytes 2097152 | tf_op jit(solution)/shard_map/reshape | solution.py:169
  23.8 2.6 %multiply_bitcast_fusion.2 = (f32[16,16,16,64]{3,2,1,0:T(8,128)}, f32[16,16,16,64]{3,2,1,0:T(8,128)}) fusion(f32[16,64,16]{1,2,0:T(8,128)S(1)} %get-tuple-element.81, f32[16,16]{1,0:T(8,128)S(1)} %fusion.78, f32[16,64,16]{1,2,0:T(8,128)S(1)} %get-tuple-element.82), kind=kLoop, calls=%fused_computation.11 | loop fusion | flops 524288 | bytes 2229248 | tf_op jit(solution)/shard_map/gnc,gh->gchn/transpose | solution.py:137
  26.3 2.0 reshape.306
  28.5 2.8 %reshape.303 = f32[256,1024]{1,0:T(8,128)} reshape(f32[16,16,16,64]{3,2,1,0:T(8,128)} %get-tuple-element.127) | data formatting | bytes 2097152 | tf_op jit(solution)/shard_map/reshape | solution.py:134
  32.8 23.6 %all-gather.2 = f32[8,2,1024]{2,1,0:T(2,128)} all-gather(f32[1,2,1024]{2,1,0:T(2,128)S(1)} %maximum_bitcast_fusion), channel_id=2, replica_groups=mesh['sp'=8,'tp'=4] {'sp'}, dimensions={0}, use_global_device_ids=true | all-gather | bytes 73728 | tf_op jit(solution)/shard_map/all_gather | solution.py:15
  56.3 1.5 reshape.308
  65.0 1.9 fusion.1
  67.0 7.2 %all-gather.12.cloned.1.call-done = bf16[3072,256]{1,0:T(8,128)(2,1)} async-done(((bf16[384,256]{1,0:T(8,128)(2,1)}), bf16[3072,256]{1,0:T(8,128)(2,1)}) %all-gather.12.cloned.1.call-update) | async-done | bytes 1572880 | tf_op jit(solution)/shard_map/all_gather | solution.py:93
  74.2 2.0 fusion.20
  76.9 1.5 slice.477
  78.4 1.5 slice.389
  79.9 1.5 slice.382
  82.1 1.6 slice.380
  83.6 1.5 slice.383
  85.1 1.8 add_add_fusion.1
  90.0 2.0 add_add_fusion.3
  94.1 1.6 slice.395
  95.7 1.6 slice.399
  97.3 1.8 add_add_fusion.5
  100.4 1.5 slice.403
  102.0 1.5 slice.407
  103.5 1.6 add_add_fusion.7
  105.1 1.5 slice.454
  106.6 1.5 slice.421
  108.0 1.4 slice.414
  109.5 1.5 slice.411
  110.9 1.5 slice.415
  112.4 1.5 add_add_fusion.9
  119.3 1.4 add_add_fusion.11
  126.1 1.5 slice_add_fusion.14
  133.0 1.5 slice.450
  137.8 1.6 slice.456
  146.0 1.6 slice.474
  156.6 2.7 %pad.126 = f32[256,1024]{1,0:T(8,128)} pad(f32[128,1024]{1,0:T(8,128)S(1)} %pad_maximum_fusion, f32[]{:T(128)} %constant.91.clone.1), padding=0_1_1x0_0_0 | pad | bytes 1572868 | tf_op jit(solution)/shard_map/pad | solution.py:145
  159.4 2.7 %pad.127 = f32[256,1024]{1,0:T(8,128)} pad(f32[128,1024]{1,0:T(8,128)S(1)} %add.689, f32[]{:T(128)} %constant.91.clone.1), padding=1_0_1x0_0_0 | pad | bytes 1572868 | tf_op jit(solution)/shard_map/pad | solution.py:145
  162.1 2.7 %pad.129 = f32[256,1024]{1,0:T(8,128)} pad(f32[128,1024]{1,0:T(8,128)S(1)} %add.692, f32[]{:T(128)} %constant.91.clone.1), padding=1_0_1x0_0_0 | pad | bytes 1572868 | tf_op jit(solution)/shard_map/pad | solution.py:145
  164.9 2.7 %pad.128 = f32[256,1024]{1,0:T(8,128)} pad(f32[128,1024]{1,0:T(8,128)S(1)} %pad_maximum_fusion.1, f32[]{:T(128)} %constant.91.clone.1), padding=0_1_1x0_0_0 | pad | bytes 1572868 | tf_op jit(solution)/shard_map/pad | solution.py:145
  169.2 22.5 %all-gather.3 = f32[8,2,1024]{2,1,0:T(2,128)S(1)} all-gather(f32[1,2,1024]{2,1,0:T(2,128)S(1)} %maximum_bitcast_fusion.1), channel_id=3, replica_groups=mesh['sp'=8,'tp'=4] {'sp'}, dimensions={0}, use_global_device_ids=true | all-gather | bytes 73728 | tf_op jit(solution)/shard_map/all_gather | solution.py:15
  191.6 5.0 %while.12 = (s32[]{:T(128)}, f32[2,1024]{1,0:T(2,128)S(1)}, s32[]{:T(128)}, f32[8,2,1024]{2,1,0:T(2,128)}, f32[8,2,1024]{2,1,0:T(2,128)S(1)}, /*index=5*/s32[]{:T(128)}, s32[]{:T(128)}, s32[]{:T(128)}, s32[]{}) while((s32[]{:T(128)}, f32[2,1024]{1,0:T(2,128)S(1)}, s32[]{:T(128)}, f32[8,2,1024]{2,1,0:T(2,128)}, f32[8,2,1024]{2,1,0:T(2,128)S(1)}, ...), condition=%wide.region_2.3_spmd, body=%wide.region_1.2_spmd.sunk | while | flops 10246 | bytes 49311 | solution.py:23
  196.8 2.1 fusion.17
  199.0 5.8 %collective-permute-start = (bf16[16,256]{1,0:T(8,128)(2,1)S(1)}, bf16[16,256]{1,0:T(8,128)(2,1)S(1)}, u32[]{:S(2)}, u32[]{:S(2)}) collective-permute-start(bf16[16,256]{1,0:T(8,128)(2,1)S(1)} %slice.534), channel_id=1, source_target_pairs={{0,4},{4,8},{8,12},{12,16},{16,20},{20,24},{24,28},{1,5},{5,9},{9,... | collective-permute-start | bytes 24584 | tf_op jit(solution)/shard_map/ppermute | solution.py:29
  204.9 5.1 %fusion.29 = f32[256,256]{1,0:T(8,128)S(1)} fusion(f32[1024,256]{0,1:T(8,128)S(1)} %copy-done.12, f32[256,1024]{1,0:T(8,128)S(1)} %copy-done.9, f32[256,1024]{1,0:T(8,128)S(1)} %copy-done.11, f32[1024]{0:T(1024)S(1)} %bitcast.64, f32[1024]{0:T(1024)S(1)} %bitcast.62, f32[1024]{0:T(1024)S(1)} %copy-done.52, f32[1024]{0:T(1024)S(1)} %copy-done.53, ...), kind=kOutput, calls=%fused_computation.39 | convolution fusion | flops 807665664 | bytes 3425280 | tf_op jit(solution)/shard_map/dot_general | solution.py:175
  210.0 5.1 %fusion.67 = bf16[256,256]{1,0:T(8,128)(2,1)S(1)} fusion(f32[256,256]{1,0:T(8,128)S(1)} %fusion.29, f32[1024,256]{0,1:T(8,128)S(1)} %copy-done.13, f32[256,1024]{1,0:T(8,128)S(1)} %copy-done.10, f32[256,1024]{1,0:T(8,128)S(1)} %copy-done.8, f32[1024]{0:T(1024)S(1)} %bitcast.65, f32[1024]{0:T(1024)S(1)} %bitcast.63, f32[1024]{0:T(1024)S(1)} %copy-done.52, ...), kind=kOutput, calls=%fused_computation.83 | convolution fusion | flops 808517632 | bytes 3688448 | tf_op jit(solution)/shard_map/dot_general | solution.py:176
  215.2 16.8 %all_gather.39 = bf16[256,1024]{1,0:T(8,128)(2,1)S(1)} all-gather(bf16[256,256]{1,0:T(8,128)(2,1)S(1)} %fusion.67), channel_id=1, replica_groups=mesh['sp'=8,'tp'=4] {'tp'}, dimensions={1}, use_global_device_ids=true | all-gather | bytes 655360 | tf_op jit(solution)/shard_map/all_gather | solution.py:210
  232.1 2.0 fusion.93
  235.8 7.3 %all_gather.42 = bf16[256,1024]{1,0:T(8,128)(2,1)S(1)} all-gather(bf16[256,256]{1,0:T(8,128)(2,1)S(1)} %fusion.16), channel_id=1, replica_groups=mesh['sp'=8,'tp'=4] {'tp'}, dimensions={1}, use_global_device_ids=true | all-gather | bytes 655360 | tf_op jit(solution)/shard_map/all_gather | solution.py:215
  243.1 2.7 %fusion.6 = bf16[256,768]{1,0:T(8,128)(2,1)} fusion(f32[256,768]{1,0:T(8,128)S(1)} %fusion.93, bf16[256,1024]{1,0:T(8,128)(2,1)S(1)} %all_gather.42, bf16[1024,768]{1,0:T(8,128)(2,1)} %all-gather.18.cloned.1.call-done), kind=kOutput, calls=%fused_computation.18 | convolution fusion | flops 403046400 | bytes 3276800 | tf_op jit(solution)/shard_map/dot_general | solution.py:214
  (307 shorter events, 72.0 us)
Async XLA Ops:
  6.5 58.5 %all-gather.10.cloned.1.call-start = ((), (), s32[]{:S(2)}) async-start(), calls=%async_computation | async-start | bytes 1966080 | tf_op jit(solution)/shard_map/all_gather | solution.py:102
  7.3 66.9 %all-gather.12.cloned.1.call-start = ((), (), s32[]{:S(2)}) async-start(), calls=%async_computation.1 | async-start | bytes 1769472 | tf_op jit(solution)/shard_map/all_gather | solution.py:93
  8.0 188.7 %all-gather.16.cloned.1.call-start = ((), (), s32[]{:S(2)}) async-start(), calls=%async_computation.3 | async-start | bytes 1769472 | tf_op jit(solution)/shard_map/all_gather | solution.py:94
  8.7 223.3 %all-gather.14.cloned.1.call-start = ((), (), s32[]{:S(2)}) async-start(), calls=%async_computation.2 | async-start | bytes 1769472 | tf_op jit(solution)/shard_map/all_gather | solution.py:95
  9.3 233.7 %all-gather.18.cloned.1.call-start = ((), (), s32[]{:S(2)}) async-start(), calls=%async_computation.4 | async-start | bytes 1769472 | tf_op jit(solution)/shard_map/all_gather | solution.py:96
  28.4 56.7 %copy-start.25 = (f32[1024]{0:T(1024)}, f32[1024]{0:T(1024)S(1)}, u32[]{:S(2)}) copy-start(f32[1024]{0:T(1024)S(1)} %reshape.305) | copy-start | bytes 12292
  28.5 56.7 %copy-start.27 = (f32[1024]{0:T(1024)}, f32[1024]{0:T(1024)S(1)}, u32[]{:S(2)}) copy-start(f32[1024]{0:T(1024)S(1)} %reshape.304) | copy-start | bytes 12292
  59.3 14.8 %copy-start.61 = (f32[3072]{0:T(1024)S(1)}, f32[3072]{0:T(1024)}, u32[]{:S(2)}) copy-start(f32[3072]{0:T(1024)} %param.19) | copy-start | bytes 36868
  63.9 26.2 %copy-start.29 = (f32[1024]{0:T(1024)}, f32[1024]{0:T(1024)S(1)}, u32[]{:S(2)}) copy-start(f32[1024]{0:T(1024)S(1)} %get-tuple-element.72) | copy-start | bytes 12292
  63.9 26.2 %copy-start.31 = (f32[1024]{0:T(1024)}, f32[1024]{0:T(1024)S(1)}, u32[]{:S(2)}) copy-start(f32[1024]{0:T(1024)S(1)} %get-tuple-element.73) | copy-start | bytes 12292
  63.9 33.5 %copy-start.33 = (f32[1024]{0:T(1024)}, f32[1024]{0:T(1024)S(1)}, u32[]{:S(2)}) copy-start(f32[1024]{0:T(1024)S(1)} %get-tuple-element.70) | copy-start | bytes 12292
  63.9 33.5 %copy-start.35 = (f32[1024]{0:T(1024)}, f32[1024]{0:T(1024)S(1)}, u32[]{:S(2)}) copy-start(f32[1024]{0:T(1024)S(1)} %get-tuple-element.71) | copy-start | bytes 12292
  63.9 39.6 %copy-start.37 = (f32[1024]{0:T(1024)}, f32[1024]{0:T(1024)S(1)}, u32[]{:S(2)}) copy-start(f32[1024]{0:T(1024)S(1)} %get-tuple-element.68) | copy-start | bytes 12292
  63.9 39.6 %copy-start.39 = (f32[1024]{0:T(1024)}, f32[1024]{0:T(1024)S(1)}, u32[]{:S(2)}) copy-start(f32[1024]{0:T(1024)S(1)} %get-tuple-element.69) | copy-start | bytes 12292
  65.0 9.1 %copy-start.6 = (bf16[256,3072]{1,0:T(8,128)(2,1)S(1)}, bf16[256,3072]{1,0:T(8,128)(2,1)}, u32[]{:S(2)}) copy-start(bf16[256,3072]{1,0:T(8,128)(2,1)} %all-gather.10.cloned.1.call-done) | copy-start | bytes 4718596
  67.0 9.2 %copy-start.59 = (f32[256]{0:T(256)}, f32[256]{0:T(256)S(1)}, u32[]{:S(2)}) copy-start(f32[256]{0:T(256)S(1)} %add_rsqrt_fusion) | copy-start | bytes 3076
  76.2 5.2 %copy-start.16 = (bf16[256,256]{1,0:T(8,128)(2,1)}, bf16[256,256]{1,0:T(8,128)(2,1)S(1)}, u32[]{:S(2)}) copy-start(bf16[256,256]{1,0:T(8,128)(2,1)S(1)} %fusion.20) | copy-start | bytes 393220
  76.9 70.7 %copy-start = (f32[256,1024]{1,0:T(8,128)}, f32[256,1024]{1,0:T(8,128)S(1)}, u32[]{:S(2)}) copy-start(f32[256,1024]{1,0:T(8,128)S(1)} %fusion.92) | copy-start | bytes 3145732
  76.9 4.5 %copy-start.2 = (f32[256,1024]{1,0:T(8,128)S(1)}, f32[256,1024]{1,0:T(8,128)}, u32[]{:S(2)}) copy-start(f32[256,1024]{1,0:T(8,128)} %reshape.303) | copy-start | bytes 3145732
  82.0 65.5 %copy-start.1 = (f32[256,1024]{1,0:T(8,128)}, f32[256,1024]{1,0:T(8,128)S(1)}, u32[]{:S(2)}) copy-start(f32[256,1024]{1,0:T(8,128)S(1)} %fusion.91) | copy-start | bytes 3145732
  145.9 5.5 %copy-start.50 = (f32[1,1024]{1,0:T(1,128)S(1)}, f32[1,1024]{1,0:T(1,128)}, u32[]{:S(2)}) copy-start(f32[1,1024]{1,0:T(1,128)} %slice.506) | copy-start | bytes 12292
  145.9 5.6 %copy-start.21 = (f32[7,1024]{1,0:T(8,128)S(1)}, f32[7,1024]{1,0:T(8,128)}, u32[]{:S(2)}) copy-start(f32[7,1024]{1,0:T(8,128)} %slice.454) | copy-start | bytes 86020
  145.9 5.6 %copy-start.22 = (f32[7,1024]{1,0:T(8,128)S(1)}, f32[7,1024]{1,0:T(8,128)}, u32[]{:S(2)}) copy-start(f32[7,1024]{1,0:T(8,128)} %slice.450) | copy-start | bytes 86020
  145.9 5.6 %copy-start.41 = (f32[1024]{0:T(1024)S(1)}, f32[1024]{0:T(1024)}, u32[]{:S(2)}) copy-start(f32[1024]{0:T(1024)} %get-tuple-element.66) | copy-start | bytes 12292
  145.9 5.6 %copy-start.42 = (f32[1024]{0:T(1024)S(1)}, f32[1024]{0:T(1024)}, u32[]{:S(2)}) copy-start(f32[1024]{0:T(1024)} %get-tuple-element.67) | copy-start | bytes 12292
  145.9 5.6 %copy-start.49 = (f32[1,1024]{1,0:T(1,128)S(1)}, f32[1,1024]{1,0:T(1,128)}, u32[]{:S(2)}) copy-start(f32[1,1024]{1,0:T(1,128)} %slice.486) | copy-start | bytes 12292
  145.9 5.8 %copy-start.48 = (f32[1,1024]{1,0:T(1,128)S(1)}, f32[1,1024]{1,0:T(1,128)}, u32[]{:S(2)}) copy-start(f32[1,1024]{1,0:T(1,128)} %slice.511) | copy-start | bytes 12292
  145.9 5.8 %copy-start.19 = (f32[15,1024]{1,0:T(8,128)S(1)}, f32[15,1024]{1,0:T(8,128)}, u32[]{:S(2)}) copy-start(f32[15,1024]{1,0:T(8,128)} %slice.460) | copy-start | bytes 184324
  145.9 5.8 %copy-start.20 = (f32[15,1024]{1,0:T(8,128)S(1)}, f32[15,1024]{1,0:T(8,128)}, u32[]{:S(2)}) copy-start(f32[15,1024]{1,0:T(8,128)} %slice.456) | copy-start | bytes 184324
  145.9 5.8 %copy-start.38 = (f32[1024]{0:T(1024)S(1)}, f32[1024]{0:T(1024)}, u32[]{:S(2)}) copy-start(f32[1024]{0:T(1024)} %copy-done.37) | copy-start | bytes 12292
  146.0 5.8 %copy-start.40 = (f32[1024]{0:T(1024)S(1)}, f32[1024]{0:T(1024)}, u32[]{:S(2)}) copy-start(f32[1024]{0:T(1024)} %copy-done.39) | copy-start | bytes 12292
  159.4 5.4 %slice-start = ((f32[256,1024]{1,0:T(8,128)}), f32[1,1024]{1,0:T(1,128)S(1)}, s32[]{:S(2)}) async-start(f32[256,1024]{1,0:T(8,128)} %copy-done), calls=%async_computation.5 | async-start | bytes 8192 | tf_op jit(solution)/shard_map/slice | solution.py:145
  159.4 5.4 %copy-start.5 = (f32[127,1024]{1,0:T(8,128)S(1)}, f32[127,1024]{1,0:T(8,128)}, u32[]{:S(2)}) copy-start(f32[127,1024]{1,0:T(8,128)} %get-tuple-element.79) | copy-start | bytes 1560580
  164.8 31.9 %copy-start.7 = (bf16[256,3072]{1,0:T(8,128)(2,1)S(1)}, bf16[256,3072]{1,0:T(8,128)(2,1)}, u32[]{:S(2)}) copy-start(bf16[256,3072]{1,0:T(8,128)(2,1)} %all-gather.10.cloned.1.call-done) | copy-start | bytes 4718596
  164.8 32.0 %copy-start.60 = (f32[256]{0:T(256)S(1)}, f32[256]{0:T(256)}, u32[]{:S(2)}) copy-start(f32[256]{0:T(256)} %copy-done.59) | copy-start | bytes 3076
  164.8 32.0 %copy-start.62 = (f32[3072]{0:T(1024)S(1)}, f32[3072]{0:T(1024)}, u32[]{:S(2)}) copy-start(f32[3072]{0:T(1024)} %param.19) | copy-start | bytes 36868
  196.7 8.1 %copy-start.9 = (f32[256,1024]{1,0:T(8,128)S(1)}, f32[256,1024]{1,0:T(8,128)}, u32[]{:S(2)}) copy-start(f32[256,1024]{1,0:T(8,128)} %pad.126) | copy-start | bytes 3145732
  196.7 8.1 %copy-start.52 = (f32[1024]{0:T(1024)S(1)}, f32[1024]{0:T(1024)}, u32[]{:S(2)}) copy-start(f32[1024]{0:T(1024)} %mul.1012) | copy-start | bytes 12292
  196.7 8.1 %copy-start.53 = (f32[1024]{0:T(1024)S(1)}, f32[1024]{0:T(1024)}, u32[]{:S(2)}) copy-start(f32[1024]{0:T(1024)} %mul.1009) | copy-start | bytes 12292
  196.7 8.1 %copy-start.69 = (f32[256]{0:T(256)S(1)}, f32[256]{0:T(256)}, u32[]{:S(2)}) copy-start(f32[256]{0:T(256)} %iota_add_fusion.4) | copy-start | bytes 3076
  196.8 8.1 %copy-start.11 = (f32[256,1024]{1,0:T(8,128)S(1)}, f32[256,1024]{1,0:T(8,128)}, u32[]{:S(2)}) copy-start(f32[256,1024]{1,0:T(8,128)} %pad.127) | copy-start | bytes 3145732
  196.8 8.1 %copy-start.12 = (f32[1024,256]{0,1:T(8,128)S(1)}, f32[1024,256]{0,1:T(8,128)}, u32[]{:S(2)}) copy-start(f32[1024,256]{0,1:T(8,128)} %reshape.307) | copy-start | bytes 3145732
  199.0 35.1 %collective-permute-start = (bf16[16,256]{1,0:T(8,128)(2,1)S(1)}, bf16[16,256]{1,0:T(8,128)(2,1)S(1)}, u32[]{:S(2)}, u32[]{:S(2)}) collective-permute-start(bf16[16,256]{1,0:T(8,128)(2,1)S(1)} %slice.534), channel_id=1, source_target_pairs={{0,4},{4,8},{8,12},{12,16},{16,20},{20,24},{24,28},{1,5},{5,9},{9,... | collective-permute-start | bytes 24584 | tf_op jit(solution)/shard_map/ppermute | solution.py:29
  204.9 5.1 %copy-start.8 = (f32[256,1024]{1,0:T(8,128)S(1)}, f32[256,1024]{1,0:T(8,128)}, u32[]{:S(2)}) copy-start(f32[256,1024]{1,0:T(8,128)} %pad.129) | copy-start | bytes 3145732
  204.9 5.1 %copy-start.10 = (f32[256,1024]{1,0:T(8,128)S(1)}, f32[256,1024]{1,0:T(8,128)}, u32[]{:S(2)}) copy-start(f32[256,1024]{1,0:T(8,128)} %pad.128) | copy-start | bytes 3145732
  204.9 5.1 %copy-start.13 = (f32[1024,256]{0,1:T(8,128)S(1)}, f32[1024,256]{0,1:T(8,128)}, u32[]{:S(2)}) copy-start(f32[1024,256]{0,1:T(8,128)} %reshape.308) | copy-start | bytes 3145732
  204.9 5.1 %copy-start.17 = (bf16[256,256]{1,0:T(8,128)(2,1)S(1)}, bf16[256,256]{1,0:T(8,128)(2,1)}, u32[]{:S(2)}) copy-start(bf16[256,256]{1,0:T(8,128)(2,1)} %copy-done.16) | copy-start | bytes 393220
  204.9 5.1 %copy-start.58 = (f32[256]{0:T(256)S(1)}, f32[256]{0:T(256)}, u32[]{:S(2)}) copy-start(f32[256]{0:T(256)} %dynamic_slice.46) | copy-start | bytes 3076
  (30 other events, 43.2 us)
Sparse Core Ops, SparseCore 0:
  8.9 21.0 all-gather.9
  32.1 42.0 all-gather.11
  76.4 42.4 all-gather.15
  120.9 42.5 all-gather.13
  165.5 42.8 all-gather.17
where the time goes:
time: 255 us; the launch traced here: 252 us
  local copies, waits for them, and re-layouts  89.1 us (35%)
  blocking collectives  70.1 us (27%)
  other arithmetic  40.2 us (16%)
  matrix products  21.9 us (9%)
  between operations  14.5 us (6%)
  waiting for transfers between devices  10.4 us (4%)
  starting transfers between devices  5.98 us (2%)
    slice x54, local copies, waits for them, and re-layouts, body(): lax.associative_scan(scan_combine, (decay_wide_real, decay_wide_imag, pus...  56.2 us
    all_gather x2, blocking collectives, prefix(): gathered = jax.tree.map(lambda a: lax.all_gather(a, axis), part)  46 us
    all_gather x1, blocking collectives, body(): lax.all_gather(state_out, 'tp', axis=1, tiled=True)  16.8 us
    add x13, other arithmetic, scan_combine(): second_decay_real * first_imag + second_decay_imag * first_real  13.6 us
    pad x28, local copies, waits for them, and re-layouts, body(): lax.associative_scan(scan_combine, (decay_wide_real, decay_wide_imag, pus...  13 us
    all_gather x1, blocking collectives, body(): lax.all_gather(pool_out, 'tp', axis=1, tiled=True)  7.28 us
    all_gather x1, waiting for transfers between devices, body(): lax.all_gather(state_in_weight, 'sp', axis=0, tiled=True)  7.19 us
    ppermute x1, starting transfers between devices, passed_along(): lax.ppermute(value, axis, [(source, source + steps) for source in range(f...  5.83 us
  transfers between devices with their start and end apart: 6, of which 1 were waited for; matrix products, arithmetic and copies ran while one was open for 58% of the time, Pallas kernels for 0%

commit v1 on v0

--- a/solution.py
+++ b/solution.py
@@ -8,6 +8,18 @@
 epsilon = 1e-06
 highest = lax.Precision.HIGHEST
 window_reach = 16
+
+
+def doubled_up(x, axis, dim):
+    ways, here, step = (lax.axis_size(axis), lax.axis_index(axis), x.shape[dim])
+    line, have = (x, 1)
+    while have < ways:
+        line = jnp.concatenate(
+            [line, lax.ppermute(line, axis, [(d, (d - have) % ways) for d in range(ways)])],
+            axis=dim,
+        )
+        have = 2 * have
+    return jnp.roll(line, here * step, axis=dim)
 
 
 def prefix(part, axis, combine, identity):
@@ -207,9 +219,7 @@
     state_rows = state_out_full
     pool_rows = pool_out_full
     running_sum = jnp.dot(
-        lax.all_gather(state_out, "tp", axis=1, tiled=True),
-        state_rows,
-        preferred_element_type=jnp.float32,
+        doubled_up(state_out, "tp", 1), state_rows, preferred_element_type=jnp.float32
     )
     combined = running_sum + jnp.dot(
         lax.all_gather(pool_out, "tp", axis=1, tiled=True),

time: 255 us -> 223 us (0.87)
  local copies, waits for them, and re-layouts: 89.1 us -> 41.1 us
  waiting for transfers between devices: 10.4 us -> 38.7 us
  blocking collectives: 70.1 us -> 54.2 us
  other arithmetic: 40.2 us -> 29.3 us
  matrix products: 21.9 us -> 29.4 us
  starting transfers between devices: 5.98 us -> 12.3 us
    slice x54, local copies, waits for them, and re-layouts: 56.2 us -> 14.4 us  [body(): lax.associative_scan(scan_combine, (decay_wide_real, decay_wide_imag, pus...]
    all_gather x1, waiting for transfers between devices: 0.02 us -> 20.1 us  [body(): lax.all_gather(pool_in_weight, 'sp', axis=0, tiled=True)]
    all_gather x1 -> x0, blocking collectives: 16.8 us -> none  [body(): lax.all_gather(state_out, 'tp', axis=1, tiled=True)]
    ppermute x0 -> x2, starting transfers between devices: none -> 9.69 us  [doubled_up(): lax.ppermute(line, axis, [(d, (d - have) % ways) for d in range(ways)])]
    add x13, other arithmetic: 13.6 us -> 5.89 us  [scan_combine(): second_decay_real * first_imag + second_decay_imag * first_real]
    ppermute x0 -> x2, waiting for transfers between devices: none -> 4.5 us  [doubled_up(): lax.ppermute(line, axis, [(d, (d - have) % ways) for d in range(ways)])]
    pad x28, local copies, waits for them, and re-layouts: 13 us -> 8.95 us  [body(): lax.associative_scan(scan_combine, (decay_wide_real, decay_wide_imag, pus...]
    dot_general x4, matrix products: 1.13 us -> 4.9 us  [body(): jnp.dot(band_mask, extended, preferred_element_type=jnp.float32)]
  transfers between devices with their start and end apart: 6 -> 8, of which waited for: 1 -> 3; matrix products, arithmetic and copies ran while one was open for 58% -> 43% of each run, Pallas kernels for 0% -> 0%
where the time goes in v1:
time: 223 us; the launch traced here: 220 us
  blocking collectives  54.2 us (24%)
  local copies, waits for them, and re-layouts  41.1 us (18%)
  waiting for transfers between devices  38.7 us (17%)
  matrix products  29.4 us (13%)
  other arithmetic  29.3 us (13%)
  between operations  14.5 us (7%)
  starting transfers between devices  12.3 us (6%)
    all_gather x2, blocking collectives, prefix(): gathered = jax.tree.map(lambda a: lax.all_gather(a, axis), part)  46.9 us
    all_gather x1, waiting for transfers between devices, body(): lax.all_gather(pool_in_weight, 'sp', axis=0, tiled=True)  20.1 us
    slice x54, local copies, waits for them, and re-layouts, body(): lax.associative_scan(scan_combine, (decay_wide_real, decay_wide_imag, pus...  14.4 us
    all_gather x1, waiting for transfers between devices, body(): lax.all_gather(state_in_weight, 'sp', axis=0, tiled=True)  10.9 us
    ppermute x2, starting transfers between devices, doubled_up(): lax.ppermute(line, axis, [(d, (d - have) % ways) for d in range(ways)])  9.69 us
    pad x28, local copies, waits for them, and re-layouts, body(): lax.associative_scan(scan_combine, (decay_wide_real, decay_wide_imag, pus...  8.95 us
    dot_general x1, matrix products, body(): readout_sum = jnp.dot(states_real, read_matrix_real, precision=highest)  7.75 us
    all_gather x1, blocking collectives, body(): lax.all_gather(pool_out, 'tp', axis=1, tiled=True)  7.28 us
  transfers between devices with their start and end apart: 8, of which 3 were waited for; matrix products, arithmetic and copies ran while one was open for 43% of the time, Pallas kernels for 0%

profile of v1, /device:TPU:25, one launch (start us, length us, event | category | flops | bytes accessed | tf_op | source)
XLA Modules:
  0.0 219.7 jit_solution(10877835517567969461)
XLA Ops:
  14.0 0.8 cosine_multiply_fusion
  16.2 0.8 multiply_subtract_fusion.2
  17.0 1.3 dynamic_slice.50
  18.3 1.3 dynamic_slice.53
  21.8 23.3 %all-gather.2 = f32[8,2,1024]{2,1,0:T(2,128)} all-gather(f32[1,2,1024]{2,1,0:T(2,128)S(1)} %maximum_bitcast_fusion), channel_id=2, replica_groups=mesh['sp'=8,'tp'=4] {'sp'}, dimensions={0}, use_global_device_ids=true | all-gather | bytes 73728 | tf_op jit(solution)/shard_map/all_gather | solution.py:27
  45.1 0.9 dynamic-slice_convert_fusion
  46.4 1.0 constant_dynamic-slice_fusion
  47.4 1.9 multiply_bitcast_fusion
  49.3 2.8 %reshape.308 = f32[1024,256]{0,1:T(8,128)} reshape(f32[16,64,16,16]{1,0,3,2:T(8,128)} %get-tuple-element.120) | data formatting | bytes 2097152 | tf_op jit(solution)/shard_map/reshape | solution.py:184
  52.0 1.6 reshape.307
  53.6 1.0 multiply_add_fusion.1
  54.6 1.9 multiply_bitcast_fusion.2
  56.5 2.7 %reshape.306 = f32[256,1024]{1,0:T(8,128)} reshape(f32[16,16,16,64]{3,2,1,0:T(8,128)} %get-tuple-element.126) | data formatting | bytes 2097152 | tf_op jit(solution)/shard_map/reshape | solution.py:149
  61.0 1.8 fusion.1
  62.9 10.9 %all-gather.12.cloned.1.call-done = bf16[3072,256]{1,0:T(8,128)(2,1)} async-done(((bf16[384,256]{1,0:T(8,128)(2,1)}), bf16[3072,256]{1,0:T(8,128)(2,1)}) %all-gather.12.cloned.1.call-update) | async-done | bytes 1572880 | tf_op jit(solution)/shard_map/all_gather | solution.py:105
  73.8 2.7 %fusion.20 = bf16[256,256]{0,1:T(8,128)(2,1)S(1)} fusion(bf16[3072,256]{1,0:T(8,128)(2,1)} %all-gather.12.cloned.1.call-done, bf16[256,3072]{1,0:T(8,128)(2,1)} %all-gather.10.cloned.1.call-done, f32[3072]{0:T(1024)S(1)} %copy-done.38, f32[256]{0:T(256)S(1)} %add_rsqrt_fusion), kind=kOutput, calls=%fused_computation.32 | convolution fusion | flops 405143552 | bytes 3290112 | tf_op jit(solution)/shard_map/dot_general | solution.py:118
  77.2 1.7 slice.477
  78.9 1.4 slice.389
  80.4 1.4 slice.382
  82.5 1.5 slice.474
  84.1 1.5 slice.383
  85.5 1.5 slice.380
  87.0 1.4 add_add_fusion.1
  92.2 0.8 add_add_fusion.5
  98.5 20.1 %all-gather.16.cloned.1.call-done = bf16[3072,256]{1,0:T(8,128)(2,1)} async-done(((bf16[384,256]{1,0:T(8,128)(2,1)}), bf16[3072,256]{1,0:T(8,128)(2,1)}) %all-gather.16.cloned.1.call-update) | async-done | bytes 1572880 | tf_op jit(solution)/shard_map/all_gather | solution.py:106
  118.6 2.2 %fusion.17 = bf16[256,256]{0,1:T(8,128)(2,1)S(1)} fusion(bf16[3072,256]{1,0:T(8,128)(2,1)} %all-gather.16.cloned.1.call-done, bf16[256,3072]{1,0:T(8,128)(2,1)S(1)} %copy-done.8, f32[3072]{0:T(1024)} %param.19, f32[256]{0:T(256)} %copy-done.37), kind=kOutput, calls=%fused_computation.31 | convolution fusion | flops 405143552 | bytes 3290112 | tf_op jit(solution)/shard_map/dot_general | solution.py:119
  121.5 2.4 %collective-permute-start.2 = (bf16[16,256]{0,1:T(8,128)(2,1)}, bf16[16,256]{0,1:T(8,128)(2,1)}, u32[]{:S(2)}, u32[]{:S(2)}) collective-permute-start(bf16[16,256]{0,1:T(8,128)(2,1)} %slice.534), channel_id=1, source_target_pairs={{0,4},{4,8},{8,12},{12,16},{16,20},{20,24},{24,28},{1,5},{5,9},{9,... | collective-permute-start | bytes 24584 | tf_op jit(solution)/shard_map/ppermute | solution.py:41
  127.1 0.9 copy-done.5
  128.2 1.2 add_add_fusion
  129.4 2.7 %pad.126 = f32[256,1024]{1,0:T(8,128)} pad(f32[128,1024]{1,0:T(8,128)S(1)} %pad_maximum_fusion, f32[]{:T(128)} %constant.109.clone.1), padding=0_1_1x0_0_0 | pad | bytes 1572868 | tf_op jit(solution)/shard_map/pad | solution.py:157
  132.3 2.7 %pad.127 = f32[256,1024]{1,0:T(8,128)} pad(f32[128,1024]{1,0:T(8,128)S(1)} %add.699, f32[]{:T(128)} %constant.109.clone.1), padding=1_0_1x0_0_0 | pad | bytes 1572868 | tf_op jit(solution)/shard_map/pad | solution.py:157
  135.0 2.7 %pad.129 = f32[256,1024]{1,0:T(8,128)} pad(f32[128,1024]{1,0:T(8,128)S(1)} %add.702, f32[]{:T(128)} %constant.109.clone.1), padding=1_0_1x0_0_0 | pad | bytes 1572868 | tf_op jit(solution)/shard_map/pad | solution.py:157
  139.3 23.6 %all-gather.3 = f32[8,2,1024]{2,1,0:T(2,128)S(1)} all-gather(f32[1,2,1024]{2,1,0:T(2,128)S(1)} %maximum_bitcast_fusion.1), channel_id=3, replica_groups=mesh['sp'=8,'tp'=4] {'sp'}, dimensions={0}, use_global_device_ids=true | all-gather | bytes 73728 | tf_op jit(solution)/shard_map/all_gather | solution.py:27
  162.9 5.0 %while.12 = (s32[]{:T(128)}, f32[2,1024]{1,0:T(2,128)S(1)}, s32[]{:T(128)}, f32[8,2,1024]{2,1,0:T(2,128)}, f32[8,2,1024]{2,1,0:T(2,128)S(1)}, /*index=5*/s32[]{:T(128)}, s32[]{:T(128)}, s32[]{:T(128)}, s32[]{}) while((s32[]{:T(128)}, f32[2,1024]{1,0:T(2,128)S(1)}, s32[]{:T(128)}, f32[8,2,1024]{2,1,0:T(2,128)}, f32[8,2,1024]{2,1,0:T(2,128)S(1)}, ...), condition=%wide.region_2.3_spmd, body=%wide.region_1.2_spmd.sunk | while | flops 10246 | bytes 49311 | solution.py:35
  163.7 0.8 multiply_subtract_fusion.23
  164.6 0.8 multiply_subtract_fusion.23
  168.0 7.7 %fusion.29 = f32[256,256]{0,1:T(8,128)S(1)} fusion(f32[1024,256]{0,1:T(8,128)} %reshape.307, f32[256,1024]{1,0:T(8,128)} %pad.126, f32[256,1024]{1,0:T(8,128)} %pad.127, f32[1024]{0:T(1024)S(1)} %bitcast.63, f32[1024]{0:T(1024)S(1)} %bitcast.61, f32[1024]{0:T(1024)S(1)} %copy-done.31, f32[1024]{0:T(1024)S(1)} %copy-done.30, f32[256]{0:T(256)S(1)} %copy-done.45), kind=kOutput, calls=%fused_computation.39 | convolution fusion | flops 807665664 | bytes 3425280 | tf_op jit(solution)/shard_map/dot_general | solution.py:187
  175.8 5.2 %constant_dynamic-update-slice_fusion.5 = (bf16[256,2048]{0,1:T(8,128)(2,1)S(1)}, bf16[256,256]{0,1:T(8,128)(2,1)S(1)}) fusion(bf16[256,256]{0,1:T(8,128)(2,1)S(1)} %fusion.20, f32[256]{0:T(256)S(1)} %copy-done.36, f32[256,256]{0,1:T(8,128)S(1)} %fusion.29, f32[1024,256]{0,1:T(8,128)S(1)} %copy-done.10, f32[256,1024]{1,0:T(8,128)S(1)} %pad.128, ...), kind=kOutput, calls=%fused_computation.142 | convolution fusion | flops 808517632 | bytes 3819520 | tf_op jit(solution)/shard_map/dot_general | solution.py:188
  181.1 8.4 %collective-permute-start = (bf16[256,256]{0,1:T(8,128)(2,1)S(1)}, bf16[256,256]{0,1:T(8,128)(2,1)S(1)}, u32[]{:S(2)}, u32[]{:S(2)}) collective-permute-start(bf16[256,256]{0,1:T(8,128)(2,1)S(1)} %get-tuple-element.129), channel_id=1, source_target_pairs={{0,3},{1,0},{2,1},{3,2},{4,7},{5,4},{6,5},{7,6},{8,11},{9,8},{10,9... | collective-permute-start | bytes 393224 | tf_op jit(solution)/shard_map/ppermute | solution.py:18
  189.5 1.2 convolution_select_fusion
  190.8 1.2 convolution_select_fusion.1
  192.1 1.2 convolution_select_fusion.2
  193.3 1.2 fusion.8
  195.2 7.3 %all_gather.38 = bf16[256,1024]{1,0:T(8,128)(2,1)S(1)} all-gather(bf16[256,256]{1,0:T(8,128)(2,1)S(1)} %fusion.16), channel_id=1, replica_groups=mesh['sp'=8,'tp'=4] {'tp'}, dimensions={1}, use_global_device_ids=true | all-gather | bytes 655360 | tf_op jit(solution)/shard_map/all_gather | solution.py:225
  202.5 1.3 collective-permute-start.1
  203.7 2.0 fusion.95
  205.7 4.5 %collective-permute-done.1 = bf16[256,512]{0,1:T(8,128)(2,1)S(1)} collective-permute-done((bf16[256,512]{0,1:T(8,128)(2,1)S(1)}, bf16[256,512]{0,1:T(8,128)(2,1)S(1)}, u32[]{:S(2)}, u32[]{:S(2)}) %collective-permute-start.1) | collective-permute-done | bytes 262176 | tf_op jit(solution)/shard_map/ppermute | solution.py:18
  210.4 2.8 %fusion.6 = bf16[256,768]{1,0:T(8,128)(2,1)} fusion(f32[256,768]{1,0:T(8,128)S(1)} %fusion.95, bf16[1024,768]{1,0:T(8,128)(2,1)} %all-gather.14.cloned.1.call-done, bf16[256,2048]{0,1:T(8,128)(2,1)S(1)} %constant_dynamic-update-slice_fusion, s32[]{:T(128)S(6)} %select_n.94), kind=kOutput, calls=%fused_computation.18 | convolution fusion | flops 403046400 | bytes 3276804 | tf_op jit(solution)/shard_map/dot_general | solution.py:221
  (268 shorter events, 33.0 us)
Async XLA Ops:
  6.5 54.5 %all-gather.10.cloned.1.call-start = ((), (), s32[]{:S(2)}) async-start(), calls=%async_computation | async-start | bytes 1966080 | tf_op jit(solution)/shard_map/all_gather | solution.py:114
  7.3 66.5 %all-gather.12.cloned.1.call-start = ((), (), s32[]{:S(2)}) async-start(), calls=%async_computation.1 | async-start | bytes 1769472 | tf_op jit(solution)/shard_map/all_gather | solution.py:105
  8.0 110.6 %all-gather.16.cloned.1.call-start = ((), (), s32[]{:S(2)}) async-start(), calls=%async_computation.3 | async-start | bytes 1769472 | tf_op jit(solution)/shard_map/all_gather | solution.py:106
  8.7 195.0 %all-gather.18.cloned.1.call-start = ((), (), s32[]{:S(2)}) async-start(), calls=%async_computation.4 | async-start | bytes 1769472 | tf_op jit(solution)/shard_map/all_gather | solution.py:108
  9.3 201.0 %all-gather.14.cloned.1.call-start = ((), (), s32[]{:S(2)}) async-start(), calls=%async_computation.2 | async-start | bytes 1769472 | tf_op jit(solution)/shard_map/all_gather | solution.py:107
  59.8 14.0 %copy-start.38 = (f32[3072]{0:T(1024)S(1)}, f32[3072]{0:T(1024)}, u32[]{:S(2)}) copy-start(f32[3072]{0:T(1024)} %param.19) | copy-start | bytes 36868
  62.8 11.0 %copy-start.37 = (f32[256]{0:T(256)}, f32[256]{0:T(256)S(1)}, u32[]{:S(2)}) copy-start(f32[256]{0:T(256)S(1)} %add_rsqrt_fusion) | copy-start | bytes 3076
  62.8 13.6 %copy-start.2 = (f32[256,1024]{1,0:T(8,128)S(1)}, f32[256,1024]{1,0:T(8,128)}, u32[]{:S(2)}) copy-start(f32[256,1024]{1,0:T(8,128)} %reshape.306) | copy-start | bytes 3145732
  77.2 4.6 %copy-start = (f32[256,1024]{1,0:T(8,128)}, f32[256,1024]{1,0:T(8,128)S(1)}, u32[]{:S(2)}) copy-start(f32[256,1024]{1,0:T(8,128)S(1)} %fusion.94) | copy-start | bytes 3145732
  82.5 4.5 %copy-start.1 = (f32[256,1024]{1,0:T(8,128)}, f32[256,1024]{1,0:T(8,128)S(1)}, u32[]{:S(2)}) copy-start(f32[256,1024]{1,0:T(8,128)S(1)} %fusion.93) | copy-start | bytes 3145732
  82.5 4.5 %copy-start.3 = (f32[128,1024]{1,0:T(8,128)S(1)}, f32[128,1024]{1,0:T(8,128)}, u32[]{:S(2)}) copy-start(f32[128,1024]{1,0:T(8,128)} %slice.389) | copy-start | bytes 1572868
  82.5 4.5 %copy-start.4 = (f32[128,1024]{1,0:T(8,128)S(1)}, f32[128,1024]{1,0:T(8,128)}, u32[]{:S(2)}) copy-start(f32[128,1024]{1,0:T(8,128)} %slice.382) | copy-start | bytes 1572868
  89.0 1.6 copy-start.11
  89.0 1.6 copy-start.13
  92.2 26.4 %copy-start.8 = (bf16[256,3072]{1,0:T(8,128)(2,1)S(1)}, bf16[256,3072]{1,0:T(8,128)(2,1)}, u32[]{:S(2)}) copy-start(bf16[256,3072]{1,0:T(8,128)(2,1)} %all-gather.10.cloned.1.call-done) | copy-start | bytes 4718596
  98.5 25.8 %copy-start.19 = (f32[1024]{0:T(1024)S(1)}, f32[1024]{0:T(1024)}, u32[]{:S(2)}) copy-start(f32[1024]{0:T(1024)} %get-tuple-element.66) | copy-start | bytes 12292
  98.5 25.8 %copy-start.20 = (f32[1024]{0:T(1024)S(1)}, f32[1024]{0:T(1024)}, u32[]{:S(2)}) copy-start(f32[1024]{0:T(1024)} %get-tuple-element.67) | copy-start | bytes 12292
  120.8 3.9 %copy-start.21 = (bf16[256,256]{0,1:T(8,128)(2,1)}, bf16[256,256]{0,1:T(8,128)(2,1)S(1)}, u32[]{:S(2)}) copy-start(bf16[256,256]{0,1:T(8,128)(2,1)S(1)} %fusion.17) | copy-start | bytes 393220
  120.8 3.8 %copy-start.17 = (f32[1024]{0:T(1024)S(1)}, f32[1024]{0:T(1024)}, u32[]{:S(2)}) copy-start(f32[1024]{0:T(1024)} %get-tuple-element.68) | copy-start | bytes 12292
  120.8 3.8 %copy-start.18 = (f32[1024]{0:T(1024)S(1)}, f32[1024]{0:T(1024)}, u32[]{:S(2)}) copy-start(f32[1024]{0:T(1024)} %get-tuple-element.69) | copy-start | bytes 12292
  120.8 3.8 %copy-start.28 = (f32[1,1024]{1,0:T(1,128)S(1)}, f32[1,1024]{1,0:T(1,128)}, u32[]{:S(2)}) copy-start(f32[1,1024]{1,0:T(1,128)} %slice.485) | copy-start | bytes 12292
  120.8 3.8 %copy-start.27 = (f32[1,1024]{1,0:T(1,128)S(1)}, f32[1,1024]{1,0:T(1,128)}, u32[]{:S(2)}) copy-start(f32[1,1024]{1,0:T(1,128)} %slice.516) | copy-start | bytes 12292
  121.5 68.0 %collective-permute-start.2 = (bf16[16,256]{0,1:T(8,128)(2,1)}, bf16[16,256]{0,1:T(8,128)(2,1)}, u32[]{:S(2)}, u32[]{:S(2)}) collective-permute-start(bf16[16,256]{0,1:T(8,128)(2,1)} %slice.534), channel_id=1, source_target_pairs={{0,4},{4,8},{8,12},{12,16},{16,20},{20,24},{24,28},{1,5},{5,9},{9,... | collective-permute-start | bytes 24584 | tf_op jit(solution)/shard_map/ppermute | solution.py:41
  127.0 1.0 copy-start.5
  127.0 1.2 copy-start.6
  128.2 1.2 slice-start.1
  129.3 2.8 %slice-start = ((f32[256,1024]{1,0:T(8,128)}), f32[1,1024]{1,0:T(1,128)S(1)}, s32[]{:S(2)}) async-start(f32[256,1024]{1,0:T(8,128)} %copy-done), calls=%async_computation.5 | async-start | bytes 8192 | tf_op jit(solution)/shard_map/slice | solution.py:157
  129.3 2.8 %copy-start.7 = (f32[127,1024]{1,0:T(8,128)S(1)}, f32[127,1024]{1,0:T(8,128)}, u32[]{:S(2)}) copy-start(f32[127,1024]{1,0:T(8,128)} %get-tuple-element.79) | copy-start | bytes 1560580
  132.3 35.6 %copy-start.30 = (f32[1024]{0:T(1024)S(1)}, f32[1024]{0:T(1024)}, u32[]{:S(2)}) copy-start(f32[1024]{0:T(1024)} %mul.1010) | copy-start | bytes 12292
  132.3 35.6 %copy-start.31 = (f32[1024]{0:T(1024)S(1)}, f32[1024]{0:T(1024)}, u32[]{:S(2)}) copy-start(f32[1024]{0:T(1024)} %mul.1013) | copy-start | bytes 12292
  132.3 35.6 %copy-start.45 = (f32[256]{0:T(256)S(1)}, f32[256]{0:T(256)}, u32[]{:S(2)}) copy-start(f32[256]{0:T(256)} %iota_add_fusion.4) | copy-start | bytes 3076
  168.0 7.8 %copy-start.9 = (f32[256,1024]{1,0:T(8,128)S(1)}, f32[256,1024]{1,0:T(8,128)}, u32[]{:S(2)}) copy-start(f32[256,1024]{1,0:T(8,128)} %pad.129) | copy-start | bytes 3145732
  168.0 7.8 %copy-start.10 = (f32[1024,256]{0,1:T(8,128)S(1)}, f32[1024,256]{0,1:T(8,128)}, u32[]{:S(2)}) copy-start(f32[1024,256]{0,1:T(8,128)} %reshape.308) | copy-start | bytes 3145732
  168.0 7.8 %copy-start.36 = (f32[256]{0:T(256)S(1)}, f32[256]{0:T(256)}, u32[]{:S(2)}) copy-start(f32[256]{0:T(256)} %dynamic_slice.50) | copy-start | bytes 3076
  175.8 13.8 %copy-start.22 = (bf16[256,256]{0,1:T(8,128)(2,1)S(1)}, bf16[256,256]{0,1:T(8,128)(2,1)}, u32[]{:S(2)}) copy-start(bf16[256,256]{0,1:T(8,128)(2,1)} %copy-done.21) | copy-start | bytes 393220
  175.8 13.7 %copy-start.34 = (s32[256]{0:T(256)S(1)}, s32[256]{0:T(256)}, u32[]{:S(2)}) copy-start(s32[256]{0:T(256)} %get-tuple-element.141) | copy-start | bytes 3076
  175.8 13.7 %copy-start.35 = (s32[256]{0:T(256)S(1)}, s32[256]{0:T(256)}, u32[]{:S(2)}) copy-start(s32[256]{0:T(256)} %get-tuple-element.140) | copy-start | bytes 3076
  175.8 13.7 %copy-start.42 = (pred[256]{0:T(512)(128)(4,1)S(1)}, pred[256]{0:T(512)(128)(4,1)}, u32[]{:S(2)}) copy-start(pred[256]{0:T(512)(128)(4,1)} %get-tuple-element.130) | copy-start | bytes 772
  175.8 15.0 %copy-start.40 = (pred[256]{0:T(512)(128)(4,1)S(1)}, pred[256]{0:T(512)(128)(4,1)}, u32[]{:S(2)}) copy-start(pred[256]{0:T(512)(128)(4,1)} %get-tuple-element.133) | copy-start | bytes 772
  175.8 15.0 %copy-start.44 = (s32[256]{0:T(256)S(1)}, s32[256]{0:T(256)}, u32[]{:S(2)}) copy-start(s32[256]{0:T(256)} %iota_add_fusion.1) | copy-start | bytes 3076
  181.0 11.0 %copy-start.41 = (pred[256]{0:T(512)(128)(4,1)S(1)}, pred[256]{0:T(512)(128)(4,1)}, u32[]{:S(2)}) copy-start(pred[256]{0:T(512)(128)(4,1)} %get-tuple-element.131) | copy-start | bytes 772
  181.1 11.0 %copy-start.43 = (s32[256]{0:T(256)S(1)}, s32[256]{0:T(256)}, u32[]{:S(2)}) copy-start(s32[256]{0:T(256)} %iota_add_fusion.2) | copy-start | bytes 3076
  181.1 12.3 %copy-start.32 = (s32[256]{0:T(256)S(1)}, s32[256]{0:T(256)}, u32[]{:S(2)}) copy-start(s32[256]{0:T(256)} %get-tuple-element.142) | copy-start | bytes 3076
  181.1 12.3 %copy-start.33 = (s32[256]{0:T(256)S(1)}, s32[256]{0:T(256)}, u32[]{:S(2)}) copy-start(s32[256]{0:T(256)} %get-tuple-element.143) | copy-start | bytes 3076
  181.1 12.3 %copy-start.39 = (pred[256]{0:T(512)(128)(4,1)S(1)}, pred[256]{0:T(512)(128)(4,1)}, u32[]{:S(2)}) copy-start(pred[256]{0:T(512)(128)(4,1)} %get-tuple-element.132) | copy-start | bytes 772
  181.1 21.4 %collective-permute-start = (bf16[256,256]{0,1:T(8,128)(2,1)S(1)}, bf16[256,256]{0,1:T(8,128)(2,1)S(1)}, u32[]{:S(2)}, u32[]{:S(2)}) collective-permute-start(bf16[256,256]{0,1:T(8,128)(2,1)S(1)} %get-tuple-element.129), channel_id=1, source_target_pairs={{0,3},{1,0},{2,1},{3,2},{4,7},{5,4},{6,5},{7,6},{8,11},{9,8},{10,9... | collective-permute-start | bytes 393224 | tf_op jit(solution)/shard_map/ppermute | solution.py:18
  192.0 2.5 %copy-start.29 = (f32[256]{0:T(256)S(1)}, f32[256]{0:T(256)}, u32[]{:S(2)}) copy-start(f32[256]{0:T(256)} %dynamic_slice.53) | copy-start | bytes 3076
  202.5 7.8 %collective-permute-start.1 = (bf16[256,512]{0,1:T(8,128)(2,1)S(1)}, bf16[256,512]{0,1:T(8,128)(2,1)S(1)}, u32[]{:S(2)}, u32[]{:S(2)}) collective-permute-start(bf16[256,512]{0,1:T(8,128)(2,1)S(1)} %pad_maximum_fusion.4), channel_id=1, source_target_pairs={{0,2},{1,3},{2,0},{3,1},{4,6},{5,7},{6,4},{7,5},{8,10},{9,11},{10,... | collective-permute-start | bytes 786440 | tf_op jit(solution)/shard_map/ppermute | solution.py:18
  (8 other events, 5.4 us)
Sparse Core Ops, SparseCore 0:
  8.9 20.9 all-gather.9
  32.1 41.6 all-gather.11
  76.0 42.5 all-gather.15
  120.6 43.2 all-gather.17
  165.9 42.4 all-gather.13
